TPU v7x, 128 devices: a whole 4x4x4 slice. The times are simulated.
128 devices in a mesh: sp: 16 (over z, x), dp: 8 (over y, core).
Axes of the slice: x: 4, y: 4, z: 4, core: 2. Of those that a mesh axis runs over, the one named last changes fastest.
Arguments:
- residual_in: bfloat16 [8, 2048, 2048], P('dp', 'sp'), may hold values from -6 to 6
- query_rows: bfloat16 [8, 2048, 1024], P('dp', 'sp'), may hold values from -40 to 40
- key_rows: bfloat16 [8, 2048, 1024], P('dp', 'sp'), may hold values from -40 to 40
- value_rows: bfloat16 [8, 2048, 1024], P('dp', 'sp'), may hold values from -6 to 6
- gate_sums: float32 [8, 16, 2048], P('dp', 'sp'), as said below
- out_weight: bfloat16 [1024, 2048], replicated, may hold values from -0.1875 to 0.1875
- mix_gain: float32 [2048], replicated, may hold values from 0.1 to 1.9
- ffn_gain: float32 [2048], replicated, may hold values from 0.1 to 1.9
- expert_ids: int32 [8, 2048, 4], P('dp', 'sp'), may hold values from 0 to 127, all different within a row; in each aligned block of 128 rows (0 to 127, 128 to 255, ..., all dimensions but the last counted through in order) at most 8 rows name the same one
- route_weights: float32 [8, 2048, 4], P('dp', 'sp'), may hold values from 0.3 to 2
- expert_gate: bfloat16 [128, 2048, 512], P(('sp', 'dp')), may hold values from -0.125 to 0.125
- expert_up: bfloat16 [128, 2048, 512], P(('sp', 'dp')), may hold values from -0.125 to 0.125
- expert_down: bfloat16 [128, 512, 2048], P(('sp', 'dp')), may hold values from -0.25 to 0.25
- shared_gate: bfloat16 [2048, 512], replicated, may hold values from -0.125 to 0.125
- shared_up: bfloat16 [2048, 512], replicated, may hold values from -0.125 to 0.125
- shared_down: bfloat16 [512, 2048], replicated, may hold values from -0.25 to 0.25
Outputs:
- result_rows: bfloat16 [8, 2048, 2048], P('dp', 'sp')
Inputs may be any that keep to these rules, and one draw needn't show every extreme that they name: `expert_ids`: each row names 4 different experts. In the rows of one device no expert is named more than 8 times, a bound that some block reaches in some devices' rows. `gate_sums`: Non-increasing along positions for every sequence and head.
All inputs are finite; a program needn't handle non-finite values.
Results may differ from a plain program's by a relative error of at most 0.0071.
Values may be sent and summed in bfloat16 or wider, within the bound.
A program may use at most 128 MiB of HBM per device.

v0:
```python
import jax
import jax.numpy as jnp
from jax import lax
from jax.sharding import PartitionSpec as P

HEAD_DIM = 64


def sent_together(arrays, axis, split_dim, concat_dim, along):
    both = jnp.concatenate(arrays, axis=along)
    out, at, gathered = (
        lax.all_to_all(both, axis, split_axis=split_dim, concat_axis=concat_dim, tiled=True),
        0,
        [],
    )
    for a in arrays:
        gathered.append(lax.slice_in_dim(out, at, at + a.shape[along], axis=along))
        at += a.shape[along]
    return tuple(gathered)


def attend(query_all, key_all, value_all, gate_sums):
    length = query_all.shape[1]
    head_count = gate_sums.shape[1]
    score_scale = HEAD_DIM ** (-0.5)
    query_heads = query_all[0].reshape(length, head_count, HEAD_DIM)
    key_heads = key_all[0].reshape(length, head_count, HEAD_DIM)
    value_heads = value_all[0].reshape(length, head_count, HEAD_DIM)
    sums_local = gate_sums[0]
    block_rows = min(512, length)
    pieces = []
    for block_index in range(length // block_rows):
        start = block_index * block_rows
        block_end = start + block_rows
        scores = (
            jnp.einsum(
                "qhd,khd->hqk",
                query_heads[start:block_end],
                key_heads[:block_end],
                preferred_element_type=jnp.float32,
            )
            * score_scale
        )
        scores = scores + sums_local[:, start:block_end, None] - sums_local[:, None, :block_end]
        causal_mask = jnp.arange(block_end)[None, :] <= jnp.arange(start, block_end)[:, None]
        scores = jnp.where(causal_mask[None], scores, -jnp.inf)
        peak = jnp.max(scores, axis=2, keepdims=True)
        weights = jnp.exp(scores - peak)
        weights = (weights / jnp.sum(weights, axis=2, keepdims=True)).astype(jnp.bfloat16)
        mixed_heads = jnp.einsum(
            "hqk,khd->qhd", weights, value_heads[:block_end], preferred_element_type=jnp.float32
        ).astype(jnp.bfloat16)
        pieces.append(mixed_heads.reshape(block_rows, head_count * HEAD_DIM))
    return jnp.concatenate(pieces, axis=0)[None]


def gated_rows(rows_in, gate_w, up_w):
    gate_rows = jnp.dot(rows_in, gate_w, preferred_element_type=jnp.float32)
    up_rows = jnp.dot(rows_in, up_w, preferred_element_type=jnp.float32)
    return (jax.nn.silu(gate_rows) * up_rows).astype(jnp.bfloat16)


def shards(
    residual_in,
    query_rows,
    key_rows,
    value_rows,
    gate_sums,
    out_weight,
    mix_gain,
    ffn_gain,
    expert_ids,
    route_weights,
    expert_gate,
    expert_up,
    expert_down,
    shared_gate,
    shared_up,
    shared_down,
):
    key_all, value_all = sent_together((key_rows, value_rows), "sp", 2, 1, 0)
    query_all = lax.all_to_all(query_rows, "sp", split_axis=2, concat_axis=1, tiled=True)
    attended = attend(query_all, key_all, value_all, gate_sums)
    returned = lax.all_to_all(attended, "sp", split_axis=1, concat_axis=2, tiled=True)
    projected = jnp.dot(returned[0], out_weight, preferred_element_type=jnp.float32)
    residual_f = residual_in[0].astype(jnp.float32)
    mixed_rows = residual_f + mix_gain * projected * lax.rsqrt(
        jnp.mean(projected * projected, axis=1, keepdims=True) + 1e-06
    )
    normed = (
        ffn_gain
        * mixed_rows
        * lax.rsqrt(jnp.mean(mixed_rows * mixed_rows, axis=1, keepdims=True) + 1e-06)
    ).astype(jnp.bfloat16)
    shared_hidden = gated_rows(normed, shared_gate, shared_up)
    shared_out = jnp.dot(shared_hidden, shared_down, preferred_element_type=jnp.float32)
    tok_count = residual_in.shape[1]
    top_count = expert_ids.shape[2]
    width = residual_in.shape[2]
    sp_count = lax.axis_size("sp")
    dp_count = lax.axis_size("dp")
    expert_count = sp_count * dp_count
    capacity = 2 * tok_count * top_count // expert_count
    expert_list = expert_ids[0].reshape(tok_count * top_count)
    one_hot = (expert_list[:, None] == jnp.arange(expert_count, dtype=jnp.int32)[None, :]).astype(
        jnp.int32
    )
    position_in = jnp.sum((jnp.cumsum(one_hot, axis=0) - one_hot) * one_hot, axis=1)
    slot_index = expert_list * capacity + position_in
    repeated = jnp.repeat(normed, top_count, axis=0)
    outgoing = (
        jnp.zeros((expert_count * capacity, width), jnp.bfloat16).at[slot_index].set(repeated)
    )
    arrived = lax.all_to_all(
        outgoing.reshape(expert_count, capacity, width),
        ("sp", "dp"),
        split_axis=0,
        concat_axis=0,
        tiled=True,
    )
    flat_rows = arrived.reshape(-1, width)
    hidden = gated_rows(flat_rows, expert_gate[0], expert_up[0])
    finished = jnp.dot(hidden, expert_down[0], preferred_element_type=jnp.float32).astype(
        jnp.bfloat16
    )
    received = lax.all_to_all(
        finished.reshape(arrived.shape), ("sp", "dp"), split_axis=0, concat_axis=0, tiled=True
    )
    picked = received.reshape(expert_count * capacity, width)[slot_index]
    picked = picked.reshape(tok_count, top_count, width).astype(jnp.float32)
    routed = jnp.sum(picked * route_weights[0][:, :, None], axis=1)
    result_rows = (mixed_rows + shared_out + routed).astype(jnp.bfloat16)
    return result_rows[None]


def solution(mesh):
    return jax.shard_map(
        shards,
        mesh=mesh,
        in_specs=(
            P("dp", "sp", None),
            P("dp", "sp", None),
            P("dp", "sp", None),
            P("dp", "sp", None),
            P("dp", "sp", None),
            P(),
            P(),
            P(),
            P("dp", "sp", None),
            P("dp", "sp", None),
            P(("sp", "dp"), None, None),
            P(("sp", "dp"), None, None),
            P(("sp", "dp"), None, None),
            P(),
            P(),
            P(),
        ),
        out_specs=P("dp", "sp", None),
        check_vma=False,
    )
```

profile of v0, /device:TPU:1, one launch (start us, length us, event | category | flops | bytes accessed | tf_op | source)
XLA Modules:
  0.0 250.5 jit_solution(5828033538453089363)
XLA Ops:
  2.0 2.2 reduce.18
  5.0 8.5 %all-to-all-start.1 = ((bf16[16,2,4096]{2,1,0:T(2,128)(2,1)}), bf16[16,2,4096]{2,1,0:T(2,128)(2,1)}, u32[]{:S(2)}, u32[]{:S(2)}) async-start(bf16[16,2,4096]{2,1,0:T(2,128)(2,1)} %reshape.330), calls=%async_computation.1 | async-start | bytes 524288 | tf_op jit(solution)/shard_map/all_to_all | solution.py:82
  18.1 2.9 %all-to-all-done.1 = bf16[16,2,4096]{2,1,0:T(2,128)(2,1)} async-done(((bf16[16,2,4096]{2,1,0:T(2,128)(2,1)}), bf16[16,2,4096]{2,1,0:T(2,128)(2,1)}, u32[]{:S(2)}, u32[]{:S(2)}) %all-to-all-start.1) | async-done | bytes 262176 | tf_op jit(solution)/shard_map/all_to_all | solution.py:82
  21.1 4.0 %all-to-all-start = ((bf16[2,128,1024]{1,0,2:T(2,128)(2,1)}), bf16[2,128,1024]{1,0,2:T(2,128)(2,1)S(1)}, u32[]{:S(2)}, u32[]{:S(2)}) async-start(bf16[2,128,1024]{1,0,2:T(2,128)(2,1)} %pad_maximum_fusion), calls=%async_computation | async-start | bytes 1048576 | tf_op jit(solution)/shard_map/all_to_all | solution.py:12
  25.9 2.2 reshape.331
  28.4 6.5 %all-to-all-done = bf16[2,128,1024]{1,0,2:T(2,128)(2,1)S(1)} async-done(((bf16[2,128,1024]{1,0,2:T(2,128)(2,1)}), bf16[2,128,1024]{1,0,2:T(2,128)(2,1)S(1)}, u32[]{:S(2)}, u32[]{:S(2)}) %all-to-all-start) | async-done | bytes 524320 | tf_op jit(solution)/shard_map/all_to_all | solution.py:12
  43.9 12.7 %reduce.19 = bf16[2048,64]{1,0:T(8,128)(2,1)} reduce(bf16[2048,1,64]{2,1,0:T(2,128)(2,1)S(1)} %bitcast.230, bf16[]{:T(256)} %broadcast.177), dimensions={1}, to_apply=%bitcast.196.reduce_sub_computation | reduce | bytes 524290
  56.6 2.1 reshape.332
  58.7 4.1 %all-to-all-start.2 = ((bf16[16,2,4096]{2,1,0:T(2,128)(2,1)}), bf16[16,2,4096]{2,1,0:T(2,128)(2,1)S(1)}, u32[]{:S(2)}, u32[]{:S(2)}) async-start(bf16[16,2,4096]{2,1,0:T(2,128)(2,1)} %reshape.332), calls=%async_computation.2 | async-start | bytes 524288 | tf_op jit(solution)/shard_map/all_to_all | solution.py:84
  64.2 6.2 %all-to-all-done.2 = bf16[16,2,4096]{2,1,0:T(2,128)(2,1)S(1)} async-done(((bf16[16,2,4096]{2,1,0:T(2,128)(2,1)}), bf16[16,2,4096]{2,1,0:T(2,128)(2,1)S(1)}, u32[]{:S(2)}, u32[]{:S(2)}) %all-to-all-start.2) | async-done | bytes 262176 | tf_op jit(solution)/shard_map/all_to_all | solution.py:84
  71.9 3.1 %multiply_reduce_fusion.2 = (f32[128]{0:T(128)S(1)}, f32[128,2048]{1,0:T(8,128)S(1)}) fusion(bf16[128,1024]{0,1:T(8,128)(2,1)S(1)} %bitcast.235, bf16[1024,2048]{1,0:T(8,128)(2,1)} %param.21), kind=kOutput, calls=%fused_computation.58 | convolution fusion | flops 537395072 | bytes 5505536 | tf_op jit(solution)/shard_map/dot_general | solution.py:85
  76.6 2.4 broadcast_in_dim.29
  79.0 4.0 %reshape.323 = bf16[512,2048]{1,0:T(8,128)(2,1)} reshape(bf16[128,4,2048]{2,1,0:T(4,128)(2,1)} %broadcast_in_dim.29) | data formatting | bytes 4194304 | tf_op jit(solution)/shard_map/reshape | solution.py:110
  82.9 7.2 %scatter_custom_fusion = bf16[1024,2048]{1,0:T(8,128)(2,1)} fusion(s32[512]{0:T(512)S(1)} %bitcast.257, bf16[512,2048]{1,0:T(8,128)(2,1)} %reshape.323, bf16[]{:T(256)} %constant.10.clone.1), kind=kCustom, calls=%fused_computation.31 | custom fusion | bytes 4194816 | tf_op jit(solution)/shard_map/scatter | solution.py:112
  90.1 62.2 %all_to_all.55 = bf16[128,8,2048]{2,1,0:T(8,128)(2,1)S(1)} all-to-all(bf16[128,8,2048]{2,1,0:T(8,128)(2,1)} %bitcast.224), channel_id=1, replica_groups=mesh['sp'=16,'dp'=8] {'sp','dp'}, dimensions={0} | all-to-all | bytes 8388608 | tf_op jit(solution)/shard_map/all_to_all | solution.py:114
  154.3 3.7 %fusion.2 = f32[1024,512]{1,0:T(8,128)} fusion(bf16[128,8,2048]{2,1,0:T(8,128)(2,1)S(1)} %all_to_all.55, bf16[1,2048,512]{2,1,0:T(8,128)(2,1)S(1)} %copy-done.13), kind=kOutput, calls=%fused_computation.4 | convolution fusion | flops 2147483648 | bytes 8388608 | tf_op jit(solution)/shard_map/dot_general | solution.py:58
  158.0 10.0 %convert_bitcast_fusion = bf16[128,8,2048]{2,1,0:T(8,128)(2,1)} fusion(bf16[1,512,2048]{2,1,0:T(8,128)(2,1)S(1)} %copy-done, f32[1024,512]{1,0:T(8,128)} %fusion.2, bf16[1,2048,512]{2,1,0:T(8,128)(2,1)} %param.27, bf16[128,8,2048]{2,1,0:T(8,128)(2,1)} %copy-done.3), kind=kOutput, calls=%fused_computation.8 | convolution fusion | flops 4300210176 | bytes 14680064 | tf_op jit(solution)/shard_map/dot_general | solution.py:123
  168.0 6.0 %all-to-all-start.4 = ((bf16[128,8,2048]{2,1,0:T(8,128)(2,1)}), bf16[128,8,2048]{2,1,0:T(8,128)(2,1)}, u32[]{:S(2)}, u32[]{:S(2)}) async-start(bf16[128,8,2048]{2,1,0:T(8,128)(2,1)} %convert_bitcast_fusion), calls=%async_computation.4 | async-start | bytes 8388608 | tf_op jit(solution)/shard_map/all_to_all | solution.py:126
  174.1 2.2 fusion.89
  176.4 50.3 %all-to-all-done.4 = bf16[128,8,2048]{2,1,0:T(8,128)(2,1)} async-done(((bf16[128,8,2048]{2,1,0:T(8,128)(2,1)}), bf16[128,8,2048]{2,1,0:T(8,128)(2,1)}, u32[]{:S(2)}, u32[]{:S(2)}) %all-to-all-start.4) | async-done | bytes 4194336 | tf_op jit(solution)/shard_map/all_to_all | solution.py:126
  226.7 8.0 %gather_fusion = bf16[512,2048]{1,0:T(8,128)(2,1)} fusion(bf16[1024,2048]{1,0:T(8,128)(2,1)} %bitcast.42, s32[1024]{0:T(1024)S(1)} %pad_clamp_fusion), kind=kCustom, calls=%fused_computation | custom fusion | bytes 4196352 | tf_op jit(solution)/shard_map/gather | solution.py:129
  234.7 4.8 %reshape.310 = f32[128,4,2048]{2,1,0:T(4,128)} reshape(bf16[512,2048]{1,0:T(8,128)(2,1)} %gather_fusion) | data formatting | bytes 6291456 | tf_op jit(solution)/shard_map/convert_element_type | solution.py:130
  239.4 6.3 %multiply_reduce_fusion = f32[128,2048]{1,0:T(8,128)} fusion(f32[128,4,2048]{2,1,0:T(4,128)} %reshape.310, f32[128,4]{1,0:T(8,128)S(1)} %copy.87), kind=kLoop, calls=%fused_computation.7 | loop fusion | flops 1835008 | bytes 5244928 | tf_op jit(solution)/shard_map/reduce_sum | solution.py:131
  245.7 4.5 %fusion.12 = bf16[1,128,2048]{2,1,0:T(8,128)(2,1)} fusion(f32[128,2048]{1,0:T(8,128)} %multiply_reduce_fusion, bf16[512,2048]{1,0:T(8,128)(2,1)} %param.31, bf16[128,2048]{1,0:T(8,128)(2,1)} %copy-done.1, bf16[2048,512]{1,0:T(8,128)(2,1)} %param.30, f32[128,512]{1,0:T(8,128)S(1)} %fusion.89, f32[128]{0:T(128)S(1)} %add_rsqrt_fusion.1, ...), kind=kOutput, calls=%fused_computation.25 | convolution fusion | flops 539099136 | bytes 8135168 | tf_op jit(solution)/shard_map/dot_general | solution.py:96
  (99 shorter events, 23.8 us)
Async XLA Ops:
  0.0 158.0 %copy-start = (bf16[1,512,2048]{2,1,0:T(8,128)(2,1)S(1)}, bf16[1,512,2048]{2,1,0:T(8,128)(2,1)}, u32[]{:S(2)}) copy-start(bf16[1,512,2048]{2,1,0:T(8,128)(2,1)} %param.28) | copy-start | bytes 6291460
  0.0 14.1 %copy-start.9 = (s32[1,128,4]{1,2,0:T(4,128)S(1)}, s32[1,128,4]{1,2,0:T(4,128)}, u32[]{:S(2)}) copy-start(s32[1,128,4]{1,2,0:T(4,128)} %param.24) | copy-start | bytes 6148
  0.0 14.8 %copy-start.4 = (bf16[1,128,1024]{2,1,0:T(8,128)(2,1)S(1)}, bf16[1,128,1024]{2,1,0:T(8,128)(2,1)}, u32[]{:S(2)}) copy-start(bf16[1,128,1024]{2,1,0:T(8,128)(2,1)} %param.18) | copy-start | bytes 786436
  0.0 15.2 %copy-start.5 = (bf16[1,128,1024]{2,1,0:T(8,128)(2,1)S(1)}, bf16[1,128,1024]{2,1,0:T(8,128)(2,1)}, u32[]{:S(2)}) copy-start(bf16[1,128,1024]{2,1,0:T(8,128)(2,1)} %param.19) | copy-start | bytes 786436
  0.0 15.6 %copy-start.7 = (f32[1,1,2048]{2,1,0:T(1,128)S(1)}, f32[1,1,2048]{2,1,0:T(1,128)}, u32[]{:S(2)}) copy-start(f32[1,1,2048]{2,1,0:T(1,128)} %param.20) | copy-start | bytes 24580
  5.0 16.1 %all-to-all-start.1 = ((bf16[16,2,4096]{2,1,0:T(2,128)(2,1)}), bf16[16,2,4096]{2,1,0:T(2,128)(2,1)}, u32[]{:S(2)}, u32[]{:S(2)}) async-start(bf16[16,2,4096]{2,1,0:T(2,128)(2,1)} %reshape.330), calls=%async_computation.1 | async-start | bytes 524288 | tf_op jit(solution)/shard_map/all_to_all | solution.py:82
  21.1 13.8 %all-to-all-start = ((bf16[2,128,1024]{1,0,2:T(2,128)(2,1)}), bf16[2,128,1024]{1,0,2:T(2,128)(2,1)S(1)}, u32[]{:S(2)}, u32[]{:S(2)}) async-start(bf16[2,128,1024]{1,0,2:T(2,128)(2,1)} %pad_maximum_fusion), calls=%async_computation | async-start | bytes 1048576 | tf_op jit(solution)/shard_map/all_to_all | solution.py:12
  35.0 1.0 copy-start.12
  43.1 20.8 %copy-start.10 = (s32[1,128,4]{1,2,0:T(4,128)S(1)}, s32[1,128,4]{1,2,0:T(4,128)}, u32[]{:S(2)}) copy-start(s32[1,128,4]{1,2,0:T(4,128)} %broadcast_multiply_fusion) | copy-start | bytes 6148
  58.7 11.8 %all-to-all-start.2 = ((bf16[16,2,4096]{2,1,0:T(2,128)(2,1)}), bf16[16,2,4096]{2,1,0:T(2,128)(2,1)S(1)}, u32[]{:S(2)}, u32[]{:S(2)}) async-start(bf16[16,2,4096]{2,1,0:T(2,128)(2,1)} %reshape.332), calls=%async_computation.2 | async-start | bytes 524288 | tf_op jit(solution)/shard_map/all_to_all | solution.py:84
  71.8 3.1 %copy-start.2 = (bf16[1,128,2048]{2,1,0:T(8,128)(2,1)S(1)}, bf16[1,128,2048]{2,1,0:T(8,128)(2,1)}, u32[]{:S(2)}) copy-start(bf16[1,128,2048]{2,1,0:T(8,128)(2,1)} %param.16) | copy-start | bytes 1572868
  71.8 3.1 %copy-start.6 = (f32[2048]{0:T(1024)S(1)}, f32[2048]{0:T(1024)}, u32[]{:S(2)}) copy-start(f32[2048]{0:T(1024)} %param.22) | copy-start | bytes 24580
  71.8 3.5 %copy-start.8 = (f32[2048]{0:T(1024)S(1)}, f32[2048]{0:T(1024)}, u32[]{:S(2)}) copy-start(f32[2048]{0:T(1024)} %param.23) | copy-start | bytes 24580
  75.7 0.8 copy-start.1
  90.1 64.2 %copy-start.13 = (bf16[1,2048,512]{2,1,0:T(8,128)(2,1)S(1)}, bf16[1,2048,512]{2,1,0:T(8,128)(2,1)}, u32[]{:S(2)}) copy-start(bf16[1,2048,512]{2,1,0:T(8,128)(2,1)} %param.26) | copy-start | bytes 6291460
  152.3 2.0 copy-start.3
  168.0 6.0 %copy-start.11 = (f32[1,128,4]{1,2,0:T(4,128)S(1)}, f32[1,128,4]{1,2,0:T(4,128)}, u32[]{:S(2)}) copy-start(f32[1,128,4]{1,2,0:T(4,128)} %param.25) | copy-start | bytes 6148
  168.0 58.7 %all-to-all-start.4 = ((bf16[128,8,2048]{2,1,0:T(8,128)(2,1)}), bf16[128,8,2048]{2,1,0:T(8,128)(2,1)}, u32[]{:S(2)}, u32[]{:S(2)}) async-start(bf16[128,8,2048]{2,1,0:T(8,128)(2,1)} %convert_bitcast_fusion), calls=%async_computation.4 | async-start | bytes 8388608 | tf_op jit(solution)/shard_map/all_to_all | solution.py:126
where the time goes:
time: 255 us; the launch traced here: 251 us
  waiting for transfers between devices  66 us (26%)
  blocking collectives  62.2 us (24%)
  local copies, waits for them, and re-layouts  41.9 us (16%)
  matrix products  28.8 us (11%)
  other arithmetic  28.3 us (11%)
  starting transfers between devices  22.6 us (9%)
    all_to_all x1, blocking collectives, shards(): lax.all_to_all(outgoing.reshape(expert_count, capacity, width), ('sp', 'd...  62.2 us
    all_to_all x1, waiting for transfers between devices, shards(): lax.all_to_all(finished.reshape(arrived.shape), ('sp', 'dp'), split_axis=...  50.3 us
    unnamed x2, other arithmetic  14.9 us
    unnamed x40, local copies, waits for them, and re-layouts  11.5 us
    dot_general x1, matrix products, shards(): jnp.dot(hidden, expert_down[0], preferred_element_type=jnp.float32)  9.96 us
    all_to_all x1, starting transfers between devices, shards(): lax.all_to_all(query_rows, 'sp', split_axis=2, concat_axis=1, tiled=True)  8.47 us
    gather x1, local copies, waits for them, and re-layouts, shards(): picked = received.reshape(expert_count * capacity, width)[slot_index]  7.96 us
    scatter x1, local copies, waits for them, and re-layouts, shards(): jnp.zeros((expert_count * capacity, width), jnp.bfloat16).at[slot_index]  7.21 us
  transfers between devices with their start and end apart: 4, of which 4 were waited for; matrix products, arithmetic and copies ran while one was open for 5% of the time, Pallas kernels for 0%

commit v1 on v0

--- a/solution.py
+++ b/solution.py
@@ -4,6 +4,15 @@
 from jax.sharding import PartitionSpec as P
 
 HEAD_DIM = 64
+
+
+def arrange_ends(mat):
+    w1 = lax.axis_size("sp")
+    a_now = jnp.split(mat, w1, axis=1)
+    z2 = jnp.stack(a_now, axis=0)
+    v_next = lax.all_to_all(z2, axis_name="sp", split_axis=0, concat_axis=0)
+    carry_out = jnp.concatenate(v_next, axis=2)
+    return carry_out
 
 
 def sent_together(arrays, axis, split_dim, concat_dim, along):
@@ -81,7 +90,7 @@
     key_all, value_all = sent_together((key_rows, value_rows), "sp", 2, 1, 0)
     query_all = lax.all_to_all(query_rows, "sp", split_axis=2, concat_axis=1, tiled=True)
     attended = attend(query_all, key_all, value_all, gate_sums)
-    returned = lax.all_to_all(attended, "sp", split_axis=1, concat_axis=2, tiled=True)
+    returned = arrange_ends(attended)
     projected = jnp.dot(returned[0], out_weight, preferred_element_type=jnp.float32)
     residual_f = residual_in[0].astype(jnp.float32)
     mixed_rows = residual_f + mix_gain * projected * lax.rsqrt(

time: 255 us -> 243 us (0.953); the launches traced: 251 us -> 242 us
  other arithmetic: 28.3 us -> 14.7 us
  local copies, waits for them, and re-layouts: 41.9 us -> 47.4 us
    unnamed x2 -> x1, other arithmetic: 14.9 us -> 2.21 us
    unnamed x40 -> x54, local copies, waits for them, and re-layouts: 11.5 us -> 17.8 us
  transfers between devices with their start and end apart: 4 -> 4, of which waited for: 4 -> 4; matrix products, arithmetic and copies ran while one was open for 5% -> 4% of each run, Pallas kernels for 0% -> 0%
where the time goes in v1:
time: 243 us; the launch traced here: 242 us
  waiting for transfers between devices  66.8 us (27%)
  blocking collectives  62 us (26%)
  local copies, waits for them, and re-layouts  47.4 us (20%)
  matrix products  28.8 us (12%)
  starting transfers between devices  21.6 us (9%)
  other arithmetic  14.7 us (6%)
    all_to_all x1, blocking collectives, shards(): lax.all_to_all(outgoing.reshape(expert_count, capacity, width), ('sp', 'd...  62 us
    all_to_all x1, waiting for transfers between devices, shards(): lax.all_to_all(finished.reshape(arrived.shape), ('sp', 'dp'), split_axis=...  50.5 us
    unnamed x54, local copies, waits for them, and re-layouts  17.8 us
    dot_general x1, matrix products, shards(): jnp.dot(hidden, expert_down[0], preferred_element_type=jnp.float32)  9.96 us
    all_to_all x1, starting transfers between devices, shards(): lax.all_to_all(query_rows, 'sp', split_axis=2, concat_axis=1, tiled=True)  8.47 us
    gather x1, local copies, waits for them, and re-layouts, shards(): picked = received.reshape(expert_count * capacity, width)[slot_index]  7.96 us
    scatter x1, local copies, waits for them, and re-layouts, shards(): jnp.zeros((expert_count * capacity, width), jnp.bfloat16).at[slot_index]  7.21 us
    all_to_all x1, waiting for transfers between devices, arrange_ends(): v_next = lax.all_to_all(z2, axis_name='sp', split_axis=0, concat_axis=0)  6.92 us
  transfers between devices with their start and end apart: 4, of which 4 were waited for; matrix products, arithmetic and copies ran while one was open for 4% of the time, Pallas kernels for 0%

profile of v1, /device:TPU:1, one launch (start us, length us, event | category | flops | bytes accessed | tf_op | source)
XLA Modules:
  0.0 241.8 jit_solution(14440088158304944297)
XLA Ops:
  2.0 2.2 reduce.18
  4.9 8.5 %all-to-all-start.1 = ((bf16[16,2,4096]{2,1,0:T(2,128)(2,1)}), bf16[16,2,4096]{2,1,0:T(2,128)(2,1)}, u32[]{:S(2)}, u32[]{:S(2)}) async-start(bf16[16,2,4096]{2,1,0:T(2,128)(2,1)} %reshape.333), calls=%async_computation.1 | async-start | bytes 524288 | tf_op jit(solution)/shard_map/all_to_all | solution.py:91
  16.0 2.0 pad_maximum_fusion
  18.1 2.9 %all-to-all-done.1 = bf16[16,2,4096]{2,1,0:T(2,128)(2,1)} async-done(((bf16[16,2,4096]{2,1,0:T(2,128)(2,1)}), bf16[16,2,4096]{2,1,0:T(2,128)(2,1)}, u32[]{:S(2)}, u32[]{:S(2)}) %all-to-all-start.1) | async-done | bytes 262176 | tf_op jit(solution)/shard_map/all_to_all | solution.py:91
  21.0 3.8 %all-to-all-start = ((bf16[2,128,1024]{1,0,2:T(2,128)(2,1)}), bf16[2,128,1024]{1,0,2:T(2,128)(2,1)S(1)}, u32[]{:S(2)}, u32[]{:S(2)}) async-start(bf16[2,128,1024]{1,0,2:T(2,128)(2,1)} %pad_maximum_fusion), calls=%async_computation | async-start | bytes 1048576 | tf_op jit(solution)/shard_map/all_to_all | solution.py:21
  25.7 2.2 reshape.334
  28.1 6.4 %all-to-all-done = bf16[2,128,1024]{1,0,2:T(2,128)(2,1)S(1)} async-done(((bf16[2,128,1024]{1,0,2:T(2,128)(2,1)}), bf16[2,128,1024]{1,0,2:T(2,128)(2,1)S(1)}, u32[]{:S(2)}, u32[]{:S(2)}) %all-to-all-start) | async-done | bytes 524320 | tf_op jit(solution)/shard_map/all_to_all | solution.py:21
  52.6 3.8 %all-to-all-start.2 = ((bf16[16,1,128,64]{2,3,1,0:T(8,128)(2,1)}), bf16[16,1,128,64]{2,3,1,0:T(8,128)(2,1)S(1)}, u32[]{:S(2)}, u32[]{:S(2)}) async-start(bf16[16,1,128,64]{2,3,1,0:T(8,128)(2,1)} %constant_dynamic-update-slice_fusion), calls=%async_computation.2 | async-start | bytes 524288 | tf_op jit(solution)/shard_map/all_to_all | solution.py:13
  56.9 6.9 %all-to-all-done.2 = bf16[16,1,128,64]{2,3,1,0:T(8,128)(2,1)S(1)} async-done(((bf16[16,1,128,64]{2,3,1,0:T(8,128)(2,1)}), bf16[16,1,128,64]{2,3,1,0:T(8,128)(2,1)S(1)}, u32[]{:S(2)}, u32[]{:S(2)}) %all-to-all-start.2) | async-done | bytes 262176 | tf_op jit(solution)/shard_map/all_to_all | solution.py:13
  63.8 3.1 %multiply_reduce_fusion.2 = (f32[128]{0:T(128)S(1)}, f32[128,2048]{1,0:T(8,128)S(1)}) fusion(bf16[128,1024]{0,1:T(8,128)(2,1)S(1)} %bitcast.288, bf16[1024,2048]{1,0:T(8,128)(2,1)} %param.21), kind=kOutput, calls=%fused_computation.58 | convolution fusion | flops 537395072 | bytes 5505536 | tf_op jit(solution)/shard_map/dot_general | solution.py:94
  68.5 2.4 broadcast_in_dim.29
  70.9 4.0 %reshape.326 = bf16[512,2048]{1,0:T(8,128)(2,1)} reshape(bf16[128,4,2048]{2,1,0:T(4,128)(2,1)} %broadcast_in_dim.29) | data formatting | bytes 4194304 | tf_op jit(solution)/shard_map/reshape | solution.py:119
  74.9 7.2 %scatter_custom_fusion = bf16[1024,2048]{1,0:T(8,128)(2,1)} fusion(s32[512]{0:T(512)S(1)} %bitcast.309, bf16[512,2048]{1,0:T(8,128)(2,1)} %reshape.326, bf16[]{:T(256)} %constant.10.clone.1), kind=kCustom, calls=%fused_computation.31 | custom fusion | bytes 4194816 | tf_op jit(solution)/shard_map/scatter | solution.py:121
  82.1 62.0 %all_to_all.45 = bf16[128,8,2048]{2,1,0:T(8,128)(2,1)S(1)} all-to-all(bf16[128,8,2048]{2,1,0:T(8,128)(2,1)} %bitcast.280), channel_id=1, replica_groups=mesh['sp'=16,'dp'=8] {'sp','dp'}, dimensions={0} | all-to-all | bytes 8388608 | tf_op jit(solution)/shard_map/all_to_all | solution.py:123
  144.1 2.0 copy-done.3
  146.1 3.7 %fusion.2 = f32[1024,512]{1,0:T(8,128)} fusion(bf16[128,8,2048]{2,1,0:T(8,128)(2,1)S(1)} %all_to_all.45, bf16[1,2048,512]{2,1,0:T(8,128)(2,1)S(1)} %copy-done.14), kind=kOutput, calls=%fused_computation.4 | convolution fusion | flops 2147483648 | bytes 8388608 | tf_op jit(solution)/shard_map/dot_general | solution.py:67
  149.8 10.0 %convert_bitcast_fusion = bf16[128,8,2048]{2,1,0:T(8,128)(2,1)} fusion(bf16[1,512,2048]{2,1,0:T(8,128)(2,1)S(1)} %copy-done, f32[1024,512]{1,0:T(8,128)} %fusion.2, bf16[1,2048,512]{2,1,0:T(8,128)(2,1)} %param.27, bf16[128,8,2048]{2,1,0:T(8,128)(2,1)} %copy-done.3), kind=kOutput, calls=%fused_computation.8 | convolution fusion | flops 4300210176 | bytes 14680064 | tf_op jit(solution)/shard_map/dot_general | solution.py:132
  159.7 5.6 %all-to-all-start.4 = ((bf16[128,8,2048]{2,1,0:T(8,128)(2,1)}), bf16[128,8,2048]{2,1,0:T(8,128)(2,1)}, u32[]{:S(2)}, u32[]{:S(2)}) async-start(bf16[128,8,2048]{2,1,0:T(8,128)(2,1)} %convert_bitcast_fusion), calls=%async_computation.4 | async-start | bytes 8388608 | tf_op jit(solution)/shard_map/all_to_all | solution.py:135
  165.5 2.2 fusion.89
  167.7 50.5 %all-to-all-done.4 = bf16[128,8,2048]{2,1,0:T(8,128)(2,1)} async-done(((bf16[128,8,2048]{2,1,0:T(8,128)(2,1)}), bf16[128,8,2048]{2,1,0:T(8,128)(2,1)}, u32[]{:S(2)}, u32[]{:S(2)}) %all-to-all-start.4) | async-done | bytes 4194336 | tf_op jit(solution)/shard_map/all_to_all | solution.py:135
  218.2 8.0 %gather_fusion = bf16[512,2048]{1,0:T(8,128)(2,1)} fusion(bf16[1024,2048]{1,0:T(8,128)(2,1)} %bitcast.58, s32[1024]{0:T(1024)S(1)} %pad_clamp_fusion), kind=kCustom, calls=%fused_computation | custom fusion | bytes 4196352 | tf_op jit(solution)/shard_map/gather | solution.py:138
  226.2 4.8 %reshape.313 = f32[128,4,2048]{2,1,0:T(4,128)} reshape(bf16[512,2048]{1,0:T(8,128)(2,1)} %gather_fusion) | data formatting | bytes 6291456 | tf_op jit(solution)/shard_map/convert_element_type | solution.py:139
  230.9 6.3 %multiply_reduce_fusion = f32[128,2048]{1,0:T(8,128)} fusion(f32[128,4,2048]{2,1,0:T(4,128)} %reshape.313, f32[128,4]{1,0:T(8,128)S(1)} %copy.60), kind=kLoop, calls=%fused_computation.7 | loop fusion | flops 1835008 | bytes 5244928 | tf_op jit(solution)/shard_map/reduce_sum | solution.py:140
  237.3 4.5 %fusion.12 = bf16[1,128,2048]{2,1,0:T(8,128)(2,1)} fusion(f32[128,2048]{1,0:T(8,128)} %multiply_reduce_fusion, bf16[512,2048]{1,0:T(8,128)(2,1)} %param.31, bf16[128,2048]{1,0:T(8,128)(2,1)} %copy-done.1, bf16[2048,512]{1,0:T(8,128)(2,1)} %param.30, f32[128,512]{1,0:T(8,128)S(1)} %fusion.89, f32[128]{0:T(128)S(1)} %add_rsqrt_fusion.1, ...), kind=kOutput, calls=%fused_computation.25 | convolution fusion | flops 539099136 | bytes 8135168 | tf_op jit(solution)/shard_map/dot_general | solution.py:105
  (110 shorter events, 26.5 us)
Async XLA Ops:
  0.0 149.8 %copy-start = (bf16[1,512,2048]{2,1,0:T(8,128)(2,1)S(1)}, bf16[1,512,2048]{2,1,0:T(8,128)(2,1)}, u32[]{:S(2)}) copy-start(bf16[1,512,2048]{2,1,0:T(8,128)(2,1)} %param.28) | copy-start | bytes 6291460
  0.0 14.0 %copy-start.10 = (s32[1,128,4]{1,2,0:T(4,128)S(1)}, s32[1,128,4]{1,2,0:T(4,128)}, u32[]{:S(2)}) copy-start(s32[1,128,4]{1,2,0:T(4,128)} %param.24) | copy-start | bytes 6148
  0.0 14.7 %copy-start.5 = (bf16[1,128,1024]{2,1,0:T(8,128)(2,1)S(1)}, bf16[1,128,1024]{2,1,0:T(8,128)(2,1)}, u32[]{:S(2)}) copy-start(bf16[1,128,1024]{2,1,0:T(8,128)(2,1)} %param.18) | copy-start | bytes 786436
  0.0 15.1 %copy-start.6 = (bf16[1,128,1024]{2,1,0:T(8,128)(2,1)S(1)}, bf16[1,128,1024]{2,1,0:T(8,128)(2,1)}, u32[]{:S(2)}) copy-start(bf16[1,128,1024]{2,1,0:T(8,128)(2,1)} %param.19) | copy-start | bytes 786436
  0.0 15.5 %copy-start.8 = (f32[1,1,2048]{2,1,0:T(1,128)S(1)}, f32[1,1,2048]{2,1,0:T(1,128)}, u32[]{:S(2)}) copy-start(f32[1,1,2048]{2,1,0:T(1,128)} %param.20) | copy-start | bytes 24580
  4.9 16.1 %all-to-all-start.1 = ((bf16[16,2,4096]{2,1,0:T(2,128)(2,1)}), bf16[16,2,4096]{2,1,0:T(2,128)(2,1)}, u32[]{:S(2)}, u32[]{:S(2)}) async-start(bf16[16,2,4096]{2,1,0:T(2,128)(2,1)} %reshape.333), calls=%async_computation.1 | async-start | bytes 524288 | tf_op jit(solution)/shard_map/all_to_all | solution.py:91
  21.0 13.5 %all-to-all-start = ((bf16[2,128,1024]{1,0,2:T(2,128)(2,1)}), bf16[2,128,1024]{1,0,2:T(2,128)(2,1)S(1)}, u32[]{:S(2)}, u32[]{:S(2)}) async-start(bf16[2,128,1024]{1,0,2:T(2,128)(2,1)} %pad_maximum_fusion), calls=%async_computation | async-start | bytes 1048576 | tf_op jit(solution)/shard_map/all_to_all | solution.py:21
  34.7 1.0 copy-start.13
  42.0 14.4 %copy-start.4 = (s32[128,4,128]{0,2,1:T(8,128)S(1)}, s32[128,4,128]{0,2,1:T(8,128)}, u32[]{:S(2)}) copy-start(s32[128,4,128]{0,2,1:T(8,128)} %copy.59) | copy-start | bytes 786436
  42.0 14.6 %copy-start.11 = (s32[1,128,4]{1,2,0:T(4,128)S(1)}, s32[1,128,4]{1,2,0:T(4,128)}, u32[]{:S(2)}) copy-start(s32[1,128,4]{1,2,0:T(4,128)} %broadcast_multiply_fusion) | copy-start | bytes 6148
  52.6 11.2 %all-to-all-start.2 = ((bf16[16,1,128,64]{2,3,1,0:T(8,128)(2,1)}), bf16[16,1,128,64]{2,3,1,0:T(8,128)(2,1)S(1)}, u32[]{:S(2)}, u32[]{:S(2)}) async-start(bf16[16,1,128,64]{2,3,1,0:T(8,128)(2,1)} %constant_dynamic-update-slice_fusion), calls=%async_computation.2 | async-start | bytes 524288 | tf_op jit(solution)/shard_map/all_to_all | solution.py:13
  63.8 3.1 %copy-start.2 = (bf16[1,128,2048]{2,1,0:T(8,128)(2,1)S(1)}, bf16[1,128,2048]{2,1,0:T(8,128)(2,1)}, u32[]{:S(2)}) copy-start(bf16[1,128,2048]{2,1,0:T(8,128)(2,1)} %param.16) | copy-start | bytes 1572868
  63.8 3.1 %copy-start.7 = (f32[2048]{0:T(1024)S(1)}, f32[2048]{0:T(1024)}, u32[]{:S(2)}) copy-start(f32[2048]{0:T(1024)} %param.22) | copy-start | bytes 24580
  63.8 3.5 %copy-start.9 = (f32[2048]{0:T(1024)S(1)}, f32[2048]{0:T(1024)}, u32[]{:S(2)}) copy-start(f32[2048]{0:T(1024)} %param.23) | copy-start | bytes 24580
  67.7 0.8 copy-start.1
  82.1 64.0 %copy-start.14 = (bf16[1,2048,512]{2,1,0:T(8,128)(2,1)S(1)}, bf16[1,2048,512]{2,1,0:T(8,128)(2,1)}, u32[]{:S(2)}) copy-start(bf16[1,2048,512]{2,1,0:T(8,128)(2,1)} %param.26) | copy-start | bytes 6291460
  144.1 2.0 copy-start.3
  159.7 5.6 %copy-start.12 = (f32[1,128,4]{1,2,0:T(4,128)S(1)}, f32[1,128,4]{1,2,0:T(4,128)}, u32[]{:S(2)}) copy-start(f32[1,128,4]{1,2,0:T(4,128)} %param.25) | copy-start | bytes 6148
  159.7 58.5 %all-to-all-start.4 = ((bf16[128,8,2048]{2,1,0:T(8,128)(2,1)}), bf16[128,8,2048]{2,1,0:T(8,128)(2,1)}, u32[]{:S(2)}, u32[]{:S(2)}) async-start(bf16[128,8,2048]{2,1,0:T(8,128)(2,1)} %convert_bitcast_fusion), calls=%async_computation.4 | async-start | bytes 8388608 | tf_op jit(solution)/shard_map/all_to_all | solution.py:135
